TPU v7x, 32 devices: a whole 2x2x4 slice. The times are simulated.
32 devices in a mesh: sp: 4 (over z), tp: 8 (over y, x, core).
Axes of the slice: x: 2, y: 2, z: 4, core: 2. Of those that a mesh axis runs over, the one named last changes fastest.
Arguments:
- activations: bfloat16 [1024, 2048], P('sp', 'tp'), may hold values from -170 to 170
- norm_gain: float32 [2048], replicated, may hold values from 0.1 to 1.9
- query_weight: bfloat16 [2048, 1536], P(None, 'tp'), may hold values from -0.125 to 0.125
- latent_weight: bfloat16 [2048, 512], P(None, 'tp'), may hold values from -0.125 to 0.125
- rope_key_weight: bfloat16 [2048, 64], replicated, may hold values from -0.125 to 0.125
- latent_gain: float32 [512], replicated, may hold values from 1.5 to 64
- expand_weight: bfloat16 [512, 2048], P(None, 'tp'), may hold values from -0.25 to 0.25
- gate_weight: bfloat16 [2048, 1024], P(None, 'tp'), may hold values from -0.125 to 0.125
- pre_weight: bfloat16 [2048, 1024], P(None, 'tp'), may hold values from -0.125 to 0.125
- value_weight: bfloat16 [2048, 1024], P(None, 'tp'), may hold values from -0.125 to 0.125
- conv_kernel: bfloat16 [3, 1024], P(None, 'tp'), may hold values from -3.5 to 3.5
- output_attend: bfloat16 [1024, 2048], P('tp'), may hold values from -0.1875 to 0.1875
- output_conv: bfloat16 [1024, 2048], P('tp'), may hold values from -0.125 to 0.125
Outputs:
- mixed: bfloat16 [1024, 2048], P(('sp', 'tp'))
- log_weight_sum: float32 [8, 1024], P('tp', 'sp')
All inputs are finite; a program needn't handle non-finite values.
Results may differ from a plain program's by a relative error of at most 0.035.
The roundings to bfloat16 on the way count: a program that leaves them out, or rounds other values in their place, can miss the bound.
Values may be sent and summed in bfloat16 or wider, within the bound.
A program may use at most 128 MiB of HBM per device.

v0:
```python
import math
import jax
import jax.numpy as jnp
from jax import lax
from jax.sharding import PartitionSpec as P

D = 2048
NOPE = 128
ROPE = 64
VDIM = 128
GRID_W = 64
EPSILON = 1e-06
ROPE_BASE = 10000.0


def with_halo(array, sides, width):
    for axis, dim in sides:
        peers, length = (lax.axis_size(axis), array.shape[dim])
        up = [(i, (i + 1) % peers) for i in range(peers - 1)]
        down = [(j, i) for i, j in up]
        last = lax.slice_in_dim(array, length - width, length, axis=dim)
        leading = lax.slice_in_dim(array, 0, width, axis=dim)
        before = lax.ppermute(last, axis, up)
        after = lax.ppermute(leading, axis, down)
        array = jnp.concatenate([before, array, after], axis=dim)
    return array


def rotate(inputs, grid_rows, grid_cols):
    quarter = inputs.shape[-1] // 4
    inverse = ROPE_BASE ** (-jnp.arange(quarter, dtype=jnp.float32) / quarter)
    row_angle = (grid_rows[:, None] * inverse)[:, None, :]
    col_angle = (grid_cols[:, None] * inverse)[:, None, :]
    part_one = inputs[..., :quarter]
    part_two = inputs[..., quarter : 2 * quarter]
    part_three = inputs[..., 2 * quarter : 3 * quarter]
    part_four = inputs[..., 3 * quarter :]
    return jnp.concatenate(
        [
            part_one * jnp.cos(row_angle) - part_two * jnp.sin(row_angle),
            part_one * jnp.sin(row_angle) + part_two * jnp.cos(row_angle),
            part_three * jnp.cos(col_angle) - part_four * jnp.sin(col_angle),
            part_three * jnp.sin(col_angle) + part_four * jnp.cos(col_angle),
        ],
        axis=-1,
    )


def conv_branch(gate_proj, pre_proj, value_proj, conv_kernel):
    pre_mix = (pre_proj * value_proj).astype(jnp.bfloat16)
    padded = with_halo(pre_mix, (("sp", 0),), 1).astype(jnp.float32)
    kernel = conv_kernel.astype(jnp.float32)
    convolved = kernel[0] * padded[:-2] + kernel[1] * padded[1:-1] + kernel[2] * padded[2:]
    return (gate_proj * convolved).astype(jnp.bfloat16)


def body(
    activations,
    norm_gain,
    query_weight,
    latent_weight,
    rope_key_weight,
    latent_gain,
    expand_weight,
    gate_weight,
    pre_weight,
    value_weight,
    conv_kernel,
    output_attend,
    output_conv,
):
    tokens_here = activations.shape[0]
    query_cols = query_weight.shape[1]
    heads_here = query_cols // (NOPE + ROPE)
    latent_cols = latent_weight.shape[1]
    channels = gate_weight.shape[1]
    joined = jnp.concatenate(
        [query_weight, latent_weight, rope_key_weight, gate_weight, pre_weight, value_weight],
        axis=1,
    )
    inputs_f32 = activations.astype(jnp.float32)
    squares = lax.psum(jnp.sum(inputs_f32 * inputs_f32, axis=1, keepdims=True), "tp")
    partial_squares = jnp.zeros((tokens_here, 1), jnp.float32)
    piece_f32 = lax.all_gather(activations, "tp", axis=1, tiled=True).astype(jnp.float32)
    scaled = (piece_f32 * norm_gain).astype(jnp.bfloat16)
    running = jnp.dot(scaled, joined, preferred_element_type=jnp.float32)
    running, folded_squares = (running, partial_squares)
    inv_rms = lax.rsqrt(squares / D + EPSILON)
    projected = running * inv_rms
    latent_end = query_cols + latent_cols
    rope_end = latent_end + ROPE
    query_proj = projected[:, :query_cols]
    latent_proj = projected[:, query_cols:latent_end]
    rope_proj = projected[:, latent_end:rope_end]
    gate_proj = projected[:, rope_end : rope_end + channels]
    pre_proj = projected[:, rope_end + channels : rope_end + 2 * channels]
    value_proj = projected[:, rope_end + 2 * channels :]
    positions = lax.axis_index("sp") * tokens_here + jnp.arange(tokens_here, dtype=jnp.int32)
    grid_rows = (positions // GRID_W).astype(jnp.float32)
    grid_cols = (positions % GRID_W).astype(jnp.float32)
    query = query_proj.reshape(tokens_here, heads_here, NOPE + ROPE)
    query = jnp.concatenate(
        [query[..., :NOPE], rotate(query[..., NOPE:], grid_rows, grid_cols)], axis=-1
    )
    query = (query * (NOPE + ROPE) ** (-0.5)).astype(jnp.bfloat16)
    query_nope = query[..., :NOPE]
    query_rope = query[..., NOPE:]
    gathered = lax.all_gather(latent_proj.astype(jnp.bfloat16), "tp", axis=1, tiled=True).astype(
        jnp.float32
    )
    latent = (
        gathered
        * lax.rsqrt(jnp.mean(gathered * gathered, axis=1, keepdims=True) + EPSILON)
        * latent_gain
    ).astype(jnp.bfloat16)
    expanded = jnp.dot(latent, expand_weight, preferred_element_type=jnp.float32).astype(
        jnp.bfloat16
    )
    rope_key = rotate(rope_proj[:, None, :], grid_rows, grid_cols)[:, 0].astype(jnp.bfloat16)
    starting = (
        jnp.full((heads_here, tokens_here), -jnp.inf, jnp.float32),
        jnp.zeros((heads_here, tokens_here), jnp.float32),
        jnp.zeros((tokens_here, heads_here, VDIM), jnp.float32),
    )
    key_piece = lax.all_gather(expanded, "sp", axis=0, tiled=True)
    rope_piece = lax.all_gather(rope_key, "sp", axis=0, tiled=True)
    piece_rows = key_piece.shape[0]
    key_block = math.gcd(piece_rows, 1024)
    split_heads = key_piece.reshape(piece_rows, heads_here, NOPE + VDIM)

    def one_block(turn_index, state):
        row_max, row_sum, running_out = state
        offset = turn_index * key_block
        block_keys = lax.dynamic_slice_in_dim(split_heads, offset, key_block, 0)
        block_rope = lax.dynamic_slice_in_dim(rope_piece, offset, key_block, 0)
        scores = jnp.einsum(
            "thd,jhd->htj", query_nope, block_keys[..., :NOPE], preferred_element_type=jnp.float32
        )
        scores = scores + jnp.einsum(
            "thd,jd->htj", query_rope, block_rope, preferred_element_type=jnp.float32
        )
        new_max = jnp.maximum(row_max, jnp.max(scores, axis=-1))
        rescale = jnp.exp(row_max - new_max)
        weights = jnp.exp(scores - new_max[..., None])
        row_sum = row_sum * rescale + jnp.sum(weights, axis=-1)
        running_out = running_out * rescale.T[..., None] + jnp.einsum(
            "htj,jhd->thd",
            weights.astype(jnp.bfloat16),
            block_keys[..., NOPE:],
            preferred_element_type=jnp.float32,
        )
        return (new_max, row_sum, running_out)

    row_max, row_sum, running_out = lax.fori_loop(0, piece_rows // key_block, one_block, starting)
    attended = (
        (running_out / row_sum.T[..., None])
        .astype(jnp.bfloat16)
        .reshape(tokens_here, heads_here * VDIM)
    )
    log_weight_sum = row_max + jnp.log(row_sum)
    conv_mixed = conv_branch(gate_proj, pre_proj, value_proj, conv_kernel)
    mixed = lax.psum_scatter(
        (
            jnp.dot(attended, output_attend, preferred_element_type=jnp.float32)
            + jnp.dot(conv_mixed, output_conv, preferred_element_type=jnp.float32)
        ).astype(jnp.bfloat16),
        "tp",
        scatter_dimension=0,
        tiled=True,
    )
    return (mixed, log_weight_sum)


def solution(mesh):
    return jax.shard_map(
        body,
        mesh=mesh,
        in_specs=(
            P("sp", "tp"),
            P(),
            P(None, "tp"),
            P(None, "tp"),
            P(),
            P(),
            P(None, "tp"),
            P(None, "tp"),
            P(None, "tp"),
            P(None, "tp"),
            P(None, "tp"),
            P("tp", None),
            P("tp", None),
        ),
        out_specs=(P(("sp", "tp"), None), P("tp", "sp")),
        check_vma=False,
    )
```

profile of v0, /device:TPU:0, one launch (start us, length us, event | category | flops | bytes accessed | tf_op | source)
XLA Modules:
  0.0 135.6 jit_solution(17453811287171782455)
XLA Ops:
  7.3 0.7 all-gather.3.cloned.1.call-update
  8.0 1.0 multiply_reduce_fusion
  9.0 1.2 copy.19
  10.3 1.3 copy.20
  11.5 1.2 copy.21
  12.8 15.2 %psum.7 = f32[256,1]{0,1:T(1,128)S(1)} all-reduce(f32[256,1]{0,1:T(1,128)S(1)} %bitcast.73), channel_id=1, replica_groups=mesh['sp'=4,'tp'=8] {'tp'}, use_global_device_ids=true, to_apply=%region_1.0 | all-reduce | flops 256 | bytes 2048 | tf_op jit(solution)/shard_map/psum | solution.py:82
  28.0 0.6 slice_bitcast_fusion.13
  28.6 0.9 constant_dynamic-update-slice_fusion.5
  29.6 0.7 constant_dynamic-update-slice_fusion.4
  30.3 0.7 constant_dynamic-update-slice_fusion.3
  31.0 0.8 constant_dynamic-update-slice_fusion.2
  31.8 0.9 constant_dynamic-update-slice_fusion.1
  32.7 0.8 constant_dynamic-update-slice_fusion
  33.5 2.7 %all-gather.3.cloned.1.call-done = bf16[256,2048]{1,0:T(8,128)(2,1)} async-done(((bf16[256,256]{1,0:T(8,128)(2,1)}), bf16[256,2048]{1,0:T(8,128)(2,1)}) %all-gather.3.cloned.1.call-update) | async-done | bytes 1048592 | tf_op jit(solution)/shard_map/all_gather | solution.py:84
  36.2 3.1 %convolution_multiply_fusion = f32[256,704]{0,1:T(8,128)S(1)} fusion(bf16[2048,704]{0,1:T(8,128)(2,1)} %constant_dynamic-update-slice_fusion, bf16[256,2048]{1,0:T(8,128)(2,1)} %all-gather.3.cloned.1.call-done, f32[2048]{0:T(1024)S(1)} %copy-done.7, f32[256]{0:T(256)S(1)} %bitcast.74), kind=kOutput, calls=%fused_computation.6 | convolution fusion | flops 739950592 | bytes 4662272 | tf_op jit(solution)/shard_map/dot_general | solution.py:86
  39.9 13.4 %all-gather = bf16[1024,1,64]{0,2,1:T(8,128)(2,1)S(1)} all-gather(bf16[256,1,64]{0,2,1:T(8,128)(2,1)S(1)} %pad_maximum_fusion), channel_id=2, replica_groups=mesh['sp'=4,'tp'=8] {'sp'}, dimensions={0}, use_global_device_ids=true | all-gather | bytes 163840 | tf_op jit(solution)/shard_map/all_gather | solution.py:126
  53.5 9.3 %all_gather.13 = bf16[256,512]{0,1:T(8,128)(2,1)S(1)} all-gather(bf16[256,64]{0,1:T(8,128)(2,1)S(1)} %slice.196), channel_id=1, replica_groups=mesh['sp'=4,'tp'=8] {'tp'}, dimensions={1}, use_global_device_ids=true | all-gather | bytes 294912 | tf_op jit(solution)/shard_map/all_gather | solution.py:108
  63.3 16.1 %all_gather.14 = bf16[1024,256]{1,0:T(8,128)(2,1)S(1)} all-gather(bf16[256,256]{1,0:T(8,128)(2,1)S(1)} %convolution_convert_fusion), channel_id=1, replica_groups=mesh['sp'=4,'tp'=8] {'sp'}, dimensions={0}, use_global_device_ids=true | all-gather | bytes 655360 | tf_op jit(solution)/shard_map/all_gather | solution.py:125
  80.5 3.7 %collective-permute-start = (bf16[1,128]{0,1:T(8,128)(2,1)S(1)}, bf16[1,128]{0,1:T(8,128)(2,1)S(1)}, u32[]{:S(2)}, u32[]{:S(2)}) collective-permute-start(bf16[1,128]{0,1:T(8,128)(2,1)S(1)} %get-tuple-element.26), channel_id=1, source_target_pairs={{0,8},{8,16},{16,24},{1,9},{9,17},{17,25},{2,10},{10,18},{18,26},{... | collective-permute-start | bytes 776 | tf_op jit(solution)/shard_map/ppermute | solution.py:23
  84.2 1.3 collective-permute-start.1
  85.5 2.4 %fusion.9 = f32[256,2048]{1,0:T(8,128)} fusion(bf16[128,2048]{1,0:T(8,128)(2,1)S(1)} %copy-done, f32[1,256,1024]{2,1,0:T(8,128)S(1)} %get-tuple-element.44, f32[256]{0:T(256)S(1)} %get-tuple-element.43, bf16[1024,1,256]{2,0,1:T(8,128)(2,1)S(1)} %bitcast.70, f32[256]{0:T(256)S(1)} %get-tuple-element.42, f32[256]{0:T(256)S(1)} %get-tuple-element.41), kind=kOutput, calls=%fused_computation.19 | convolution fusion | flops 201949184 | bytes 3935232 | tf_op jit(solution)/shard_map/dot_general | solution.py:164
  88.0 2.1 %collective-permute-done.1 = bf16[1,128]{0,1:T(8,128)(2,1)S(1)} collective-permute-done((bf16[1,128]{0,1:T(8,128)(2,1)S(1)}, bf16[1,128]{0,1:T(8,128)(2,1)S(1)}, u32[]{:S(2)}, u32[]{:S(2)}) %collective-permute-start.1) | collective-permute-done | bytes 288 | tf_op jit(solution)/shard_map/ppermute | solution.py:24
  90.2 3.2 %fusion = bf16[256,2048]{1,0:T(8,128)(2,1)} fusion(f32[256,2048]{1,0:T(8,128)} %fusion.9, bf16[128,2048]{1,0:T(8,128)(2,1)S(1)} %copy-done.2, f32[258,128]{0,1:T(8,128)S(1)} %maximum_convert_fusion, f32[256,704]{0,1:T(8,128)S(1)} %convolution_multiply_fusion, f32[128]{0:T(128)} %get-tuple-element.38, f32[128]{0:T(128)} %get-tuple-element.39, ...), kind=kOutput, calls=%fused_computation.1 | convolution fusion | flops 135495680 | bytes 4195840 | tf_op jit(solution)/shard_map/dot_general | solution.py:165
  94.0 34.8 %reduce-scatter.2.cloned.1.call-done = bf16[32,2048]{1,0:T(8,128)(2,1)} async-done(((bf16[256,2048]{1,0:T(8,128)(2,1)}), bf16[32,2048]{1,0:T(8,128)(2,1)}) %reduce-scatter.2.cloned.1.call-update) | async-done | bytes 131088 | tf_op jit(solution)/shard_map/reduce_scatter | solution.py:162
  (47 shorter events, 3.2 us)
Async XLA Ops:
  7.2 78.4 %copy-start = (bf16[128,2048]{1,0:T(8,128)(2,1)S(1)}, bf16[128,2048]{1,0:T(8,128)(2,1)}, u32[]{:S(2)}) copy-start(bf16[128,2048]{1,0:T(8,128)(2,1)} %param.24) | copy-start | bytes 1572868
  7.2 20.8 %copy-start.5 = (bf16[3,128]{1,0:T(4,128)(2,1)S(1)}, bf16[3,128]{1,0:T(4,128)(2,1)}, u32[]{:S(2)}) copy-start(bf16[3,128]{1,0:T(4,128)(2,1)} %param.23) | copy-start | bytes 2308
  7.2 21.4 %copy-start.1 = (bf16[2048,192]{0,1:T(8,128)(2,1)S(1)}, bf16[2048,192]{0,1:T(8,128)(2,1)}, u32[]{:S(2)}) copy-start(bf16[2048,192]{0,1:T(8,128)(2,1)} %param.15) | copy-start | bytes 2359300
  7.2 22.3 %copy-start.3 = (bf16[2048,64]{0,1:T(8,128)(2,1)S(1)}, bf16[2048,64]{0,1:T(8,128)(2,1)}, u32[]{:S(2)}) copy-start(bf16[2048,64]{0,1:T(8,128)(2,1)} %param.16) | copy-start | bytes 786436
  7.2 23.1 %copy-start.4 = (bf16[2048,64]{0,1:T(8,128)(2,1)S(1)}, bf16[2048,64]{0,1:T(8,128)(2,1)}, u32[]{:S(2)}) copy-start(bf16[2048,64]{0,1:T(8,128)(2,1)} %param.17) | copy-start | bytes 786436
  7.2 29.0 %all-gather.3.cloned.1.call-start = ((), (), s32[]{:S(2)}) async-start(), calls=%async_computation.1 | async-start | bytes 1179648 | tf_op jit(solution)/shard_map/all_gather | solution.py:84
  8.0 120.8 %reduce-scatter.2.cloned.1.call-start = ((), (), s32[]{:S(2)}) async-start(), calls=%async_computation.2 | async-start | bytes 1179648 | tf_op jit(solution)/shard_map/reduce_scatter | solution.py:162
  28.6 7.6 %copy-start.7 = (f32[2048]{0:T(1024)S(1)}, f32[2048]{0:T(1024)}, u32[]{:S(2)}) copy-start(f32[2048]{0:T(1024)} %param.14) | copy-start | bytes 24580
  36.2 26.7 %copy-start.6 = (bf16[512,256]{1,0:T(8,128)(2,1)S(1)}, bf16[512,256]{1,0:T(8,128)(2,1)}, u32[]{:S(2)}) copy-start(bf16[512,256]{1,0:T(8,128)(2,1)} %param.19) | copy-start | bytes 786436
  36.2 26.7 %copy-start.8 = (f32[512]{0:T(512)S(1)}, f32[512]{0:T(512)}, u32[]{:S(2)}) copy-start(f32[512]{0:T(512)} %param.18) | copy-start | bytes 6148
  80.1 10.0 %copy-start.2 = (bf16[128,2048]{1,0:T(8,128)(2,1)S(1)}, bf16[128,2048]{1,0:T(8,128)(2,1)}, u32[]{:S(2)}) copy-start(bf16[128,2048]{1,0:T(8,128)(2,1)} %param.25) | copy-start | bytes 1572868
  80.5 7.4 %collective-permute-start = (bf16[1,128]{0,1:T(8,128)(2,1)S(1)}, bf16[1,128]{0,1:T(8,128)(2,1)S(1)}, u32[]{:S(2)}, u32[]{:S(2)}) collective-permute-start(bf16[1,128]{0,1:T(8,128)(2,1)S(1)} %get-tuple-element.26), channel_id=1, source_target_pairs={{0,8},{8,16},{16,24},{1,9},{9,17},{17,25},{2,10},{10,18},{18,26},{... | collective-permute-start | bytes 776 | tf_op jit(solution)/shard_map/ppermute | solution.py:23
  84.2 5.8 %collective-permute-start.1 = (bf16[1,128]{0,1:T(8,128)(2,1)S(1)}, bf16[1,128]{0,1:T(8,128)(2,1)S(1)}, u32[]{:S(2)}, u32[]{:S(2)}) collective-permute-start(bf16[1,128]{0,1:T(8,128)(2,1)S(1)} %get-tuple-element.36), channel_id=1, source_target_pairs={{8,0},{16,8},{24,16},{9,1},{17,9},{25,17},{10,2},{18,10},{26,18},{... | collective-permute-start | bytes 776 | tf_op jit(solution)/shard_map/ppermute | solution.py:24
Sparse Core Ops, SparseCore 0:
  9.9 26.2 all-gather.2
  93.5 35.1 reduce-scatter.1
where the time goes:
time: 136 us
  blocking collectives  53.9 us (40%)
  waiting for transfers between devices  40.2 us (30%)
  between operations  14.3 us (11%)
  matrix products  9.9 us (7%)
  local copies, waits for them, and re-layouts  9.39 us (7%)
  starting transfers between devices  5.04 us (4%)
  other arithmetic  2.83 us (2%)
    reduce_scatter x1, waiting for transfers between devices, body(): lax.psum_scatter((jnp.dot(attended, output_attend, preferred_element_type...  34.8 us
    all_gather x1, blocking collectives, body(): key_piece = lax.all_gather(expanded, 'sp', axis=0, tiled=True)  16.1 us
    psum x1, blocking collectives, body(): lax.psum(jnp.sum(inputs_f32 * inputs_f32, axis=1, keepdims=True), 'tp')  15.2 us
    all_gather x1, blocking collectives, body(): rope_piece = lax.all_gather(rope_key, 'sp', axis=0, tiled=True)  13.4 us
    all_gather x1, blocking collectives, body(): lax.all_gather(latent_proj.astype(jnp.bfloat16), 'tp', axis=1, tiled=True)  9.26 us
    unnamed x27, local copies, waits for them, and re-layouts  7.86 us
    ppermute x1, starting transfers between devices, with_halo(): before = lax.ppermute(last, axis, up)  3.67 us
    dot_general x1, matrix products, body(): jnp.dot(conv_mixed, output_conv, preferred_element_type=jnp.float32)  3.22 us
  transfers between devices with their start and end apart: 4, of which 3 were waited for; matrix products, arithmetic and copies ran while one was open for 10% of the time, Pallas kernels for 0%

commit v1 on v0

--- a/solution.py
+++ b/solution.py
@@ -123,7 +123,12 @@
         jnp.zeros((tokens_here, heads_here, VDIM), jnp.float32),
     )
     key_piece = lax.all_gather(expanded, "sp", axis=0, tiled=True)
-    rope_piece = lax.all_gather(rope_key, "sp", axis=0, tiled=True)
+    ring = [rope_key]
+    for hop in range(3):
+        ring.append(lax.ppermute(ring[-1], "sp", [(dev, (dev + 1) % 4) for dev in range(4)]))
+    rope_piece = jnp.roll(
+        jnp.concatenate(ring[::-1], axis=0), (lax.axis_index("sp") + 1) * ring[0].shape[0], axis=0
+    )
     piece_rows = key_piece.shape[0]
     key_block = math.gcd(piece_rows, 1024)
     split_heads = key_piece.reshape(piece_rows, heads_here, NOPE + VDIM)

time: 136 us -> 131 us (0.963)
  blocking collectives: 53.9 us -> 40.2 us
  waiting for transfers between devices: 40.2 us -> 45.6 us
  starting transfers between devices: 5.04 us -> 8.32 us
    all_gather x1 -> x0, blocking collectives: 13.4 us -> none  [body(): rope_piece = lax.all_gather(rope_key, 'sp', axis=0, tiled=True)]
    ppermute x0 -> x3, waiting for transfers between devices: none -> 9.4 us  [body(): lax.ppermute(ring[-1], 'sp', [(dev, (dev + 1) % 4) for dev in range(4)])]
    ppermute x0 -> x3, starting transfers between devices: none -> 4.24 us  [body(): lax.ppermute(ring[-1], 'sp', [(dev, (dev + 1) % 4) for dev in range(4)])]
    ppermute x1, waiting for transfers between devices: 2.06 us -> 0.01 us  [with_halo(): after = lax.ppermute(leading, axis, down)]
    reduce_scatter x1, waiting for transfers between devices: 34.8 us -> 32.8 us  [body(): lax.psum_scatter((jnp.dot(attended, output_attend, preferred_element_type...]
    unnamed x27 -> x33, local copies, waits for them, and re-layouts: 7.86 us -> 7.88 us
  transfers between devices with their start and end apart: 4 -> 7, of which waited for: 3 -> 4; matrix products, arithmetic and copies ran while one was open for 10% -> 9% of each run, Pallas kernels for 0% -> 0%
where the time goes in v1:
time: 131 us
  waiting for transfers between devices  45.6 us (35%)
  blocking collectives  40.2 us (31%)
  between operations  14.4 us (11%)
  matrix products  9.9 us (8%)
  local copies, waits for them, and re-layouts  9.37 us (7%)
  starting transfers between devices  8.32 us (6%)
  other arithmetic  2.84 us (2%)
    reduce_scatter x1, waiting for transfers between devices, body(): lax.psum_scatter((jnp.dot(attended, output_attend, preferred_element_type...  32.8 us
    all_gather x1, blocking collectives, body(): key_piece = lax.all_gather(expanded, 'sp', axis=0, tiled=True)  15.8 us
    psum x1, blocking collectives, body(): lax.psum(jnp.sum(inputs_f32 * inputs_f32, axis=1, keepdims=True), 'tp')  15.2 us
    ppermute x3, waiting for transfers between devices, body(): lax.ppermute(ring[-1], 'sp', [(dev, (dev + 1) % 4) for dev in range(4)])  9.4 us
    all_gather x1, blocking collectives, body(): lax.all_gather(latent_proj.astype(jnp.bfloat16), 'tp', axis=1, tiled=True)  9.26 us
    unnamed x33, local copies, waits for them, and re-layouts  7.88 us
    ppermute x3, starting transfers between devices, body(): lax.ppermute(ring[-1], 'sp', [(dev, (dev + 1) % 4) for dev in range(4)])  4.24 us
    dot_general x1, matrix products, body(): jnp.dot(conv_mixed, output_conv, preferred_element_type=jnp.float32)  3.21 us
  transfers between devices with their start and end apart: 7, of which 4 were waited for; matrix products, arithmetic and copies ran while one was open for 9% of the time, Pallas kernels for 0%

profile of v1, /device:TPU:0, one launch (start us, length us, event | category | flops | bytes accessed | tf_op | source)
XLA Modules:
  0.0 130.5 jit_solution(1879229346890879437)
XLA Ops:
  8.0 1.0 multiply_reduce_fusion
  9.1 1.2 copy.19
  10.3 1.3 copy.20
  11.6 1.2 copy.21
  12.8 15.2 %psum.7 = f32[256,1]{0,1:T(1,128)S(1)} all-reduce(f32[256,1]{0,1:T(1,128)S(1)} %bitcast.74), channel_id=1, replica_groups=mesh['sp'=4,'tp'=8] {'tp'}, use_global_device_ids=true, to_apply=%region_1.0 | all-reduce | flops 256 | bytes 2048 | tf_op jit(solution)/shard_map/psum | solution.py:82
  28.6 0.9 constant_dynamic-update-slice_fusion.5
  29.5 0.7 constant_dynamic-update-slice_fusion.4
  30.3 0.7 constant_dynamic-update-slice_fusion.3
  31.0 0.8 constant_dynamic-update-slice_fusion.2
  31.8 0.8 constant_dynamic-update-slice_fusion.1
  32.7 0.8 constant_dynamic-update-slice_fusion
  33.5 2.7 %all-gather.2.cloned.1.call-done = bf16[256,2048]{1,0:T(8,128)(2,1)} async-done(((bf16[256,256]{1,0:T(8,128)(2,1)}), bf16[256,2048]{1,0:T(8,128)(2,1)}) %all-gather.2.cloned.1.call-update) | async-done | bytes 1048592 | tf_op jit(solution)/shard_map/all_gather | solution.py:84
  36.2 3.1 %convolution_multiply_fusion = f32[256,704]{0,1:T(8,128)S(1)} fusion(bf16[2048,704]{0,1:T(8,128)(2,1)} %constant_dynamic-update-slice_fusion, bf16[256,2048]{1,0:T(8,128)(2,1)} %all-gather.2.cloned.1.call-done, f32[2048]{0:T(1024)S(1)} %copy-done.7, f32[256]{0:T(256)S(1)} %bitcast.75), kind=kOutput, calls=%fused_computation.6 | convolution fusion | flops 739950592 | bytes 4662272 | tf_op jit(solution)/shard_map/dot_general | solution.py:86
  39.9 1.5 %collective-permute-start = (bf16[256,64]{0,1:T(8,128)(2,1)S(1)}, bf16[256,64]{0,1:T(8,128)(2,1)S(1)}, u32[]{:S(2)}, u32[]{:S(2)}) collective-permute-start(bf16[256,64]{0,1:T(8,128)(2,1)S(1)} %maximum_bitcast_fusion), channel_id=1, source_target_pairs={{0,8},{8,16},{16,24},{24,0},{1,9},{9,17},{17,25},{25,1},{2,10},{10... | collective-permute-start | bytes 98312 | tf_op jit(solution)/shard_map/ppermute | solution.py:128
  41.6 9.3 %all_gather.10 = bf16[256,512]{0,1:T(8,128)(2,1)S(1)} all-gather(bf16[256,64]{0,1:T(8,128)(2,1)S(1)} %slice.196), channel_id=1, replica_groups=mesh['sp'=4,'tp'=8] {'tp'}, dimensions={1}, use_global_device_ids=true | all-gather | bytes 294912 | tf_op jit(solution)/shard_map/all_gather | solution.py:108
  51.5 15.8 %all_gather.11 = bf16[1024,256]{1,0:T(8,128)(2,1)S(1)} all-gather(bf16[256,256]{1,0:T(8,128)(2,1)S(1)} %convolution_convert_fusion), channel_id=1, replica_groups=mesh['sp'=4,'tp'=8] {'sp'}, dimensions={0}, use_global_device_ids=true | all-gather | bytes 655360 | tf_op jit(solution)/shard_map/all_gather | solution.py:125
  67.3 2.7 %collective-permute-start.3 = (bf16[1,128]{0,1:T(8,128)(2,1)S(1)}, bf16[1,128]{0,1:T(8,128)(2,1)S(1)}, u32[]{:S(2)}, u32[]{:S(2)}) collective-permute-start(bf16[1,128]{0,1:T(8,128)(2,1)S(1)} %get-tuple-element.26), channel_id=1, source_target_pairs={{0,8},{8,16},{16,24},{1,9},{9,17},{17,25},{2,10},{10,18},{18,26},{... | collective-permute-start | bytes 776 | tf_op jit(solution)/shard_map/ppermute | solution.py:23
  70.0 1.3 collective-permute-start.4
  71.3 2.7 %collective-permute-start.1 = (bf16[256,64]{0,1:T(8,128)(2,1)S(1)}, bf16[256,64]{0,1:T(8,128)(2,1)S(1)}, u32[]{:S(2)}, u32[]{:S(2)}) collective-permute-start(bf16[256,64]{0,1:T(8,128)(2,1)S(1)} %collective-permute-done), channel_id=1, source_target_pairs={{0,8},{8,16},{16,24},{24,0},{1,9},{9,17},{17,25},{25,1},{2,10},{10... | collective-permute-start | bytes 98312 | tf_op jit(solution)/shard_map/ppermute | solution.py:128
  74.3 3.8 %collective-permute-done.1 = bf16[256,64]{0,1:T(8,128)(2,1)S(1)} collective-permute-done((bf16[256,64]{0,1:T(8,128)(2,1)S(1)}, bf16[256,64]{0,1:T(8,128)(2,1)S(1)}, u32[]{:S(2)}, u32[]{:S(2)}) %collective-permute-start.1) | collective-permute-done | bytes 32800 | tf_op jit(solution)/shard_map/ppermute | solution.py:128
  78.2 5.6 %collective-permute-done.2 = bf16[256,64]{0,1:T(8,128)(2,1)S(1)} collective-permute-done((bf16[256,64]{0,1:T(8,128)(2,1)S(1)}, bf16[256,64]{0,1:T(8,128)(2,1)S(1)}, u32[]{:S(2)}, u32[]{:S(2)}) %collective-permute-start.2) | collective-permute-done | bytes 32800 | tf_op jit(solution)/shard_map/ppermute | solution.py:128
  84.7 2.4 %fusion.9 = f32[256,2048]{1,0:T(8,128)} fusion(bf16[128,2048]{1,0:T(8,128)(2,1)S(1)} %copy-done, f32[1,256,1024]{2,1,0:T(8,128)S(1)} %get-tuple-element.44, f32[256]{0:T(256)S(1)} %get-tuple-element.43, bf16[1024,1,256]{2,0,1:T(8,128)(2,1)S(1)} %bitcast.71, f32[256]{0:T(256)S(1)} %get-tuple-element.42, f32[256]{0:T(256)S(1)} %get-tuple-element.41), kind=kOutput, calls=%fused_computation.19 | convolution fusion | flops 201949184 | bytes 3935232 | tf_op jit(solution)/shard_map/dot_general | solution.py:169
  87.1 3.2 %fusion = bf16[256,2048]{1,0:T(8,128)(2,1)} fusion(f32[256,2048]{1,0:T(8,128)} %fusion.9, bf16[128,2048]{1,0:T(8,128)(2,1)S(1)} %copy-done.2, f32[258,128]{0,1:T(8,128)S(1)} %maximum_convert_fusion, f32[256,704]{0,1:T(8,128)S(1)} %convolution_multiply_fusion, f32[128]{0:T(128)} %get-tuple-element.38, f32[128]{0:T(128)} %get-tuple-element.39, ...), kind=kOutput, calls=%fused_computation.1 | convolution fusion | flops 135495680 | bytes 4195840 | tf_op jit(solution)/shard_map/dot_general | solution.py:170
  90.9 32.8 %reduce-scatter.2.cloned.1.call-done = bf16[32,2048]{1,0:T(8,128)(2,1)} async-done(((bf16[256,2048]{1,0:T(8,128)(2,1)}), bf16[32,2048]{1,0:T(8,128)(2,1)}) %reduce-scatter.2.cloned.1.call-update) | async-done | bytes 131088 | tf_op jit(solution)/shard_map/reduce_scatter | solution.py:167
  (60 shorter events, 4.5 us)
Async XLA Ops:
  7.2 77.5 %copy-start = (bf16[128,2048]{1,0:T(8,128)(2,1)S(1)}, bf16[128,2048]{1,0:T(8,128)(2,1)}, u32[]{:S(2)}) copy-start(bf16[128,2048]{1,0:T(8,128)(2,1)} %param.24) | copy-start | bytes 1572868
  7.2 20.8 %copy-start.5 = (bf16[3,128]{1,0:T(4,128)(2,1)S(1)}, bf16[3,128]{1,0:T(4,128)(2,1)}, u32[]{:S(2)}) copy-start(bf16[3,128]{1,0:T(4,128)(2,1)} %param.23) | copy-start | bytes 2308
  7.2 21.4 %copy-start.1 = (bf16[2048,192]{0,1:T(8,128)(2,1)S(1)}, bf16[2048,192]{0,1:T(8,128)(2,1)}, u32[]{:S(2)}) copy-start(bf16[2048,192]{0,1:T(8,128)(2,1)} %param.15) | copy-start | bytes 2359300
  7.2 22.3 %copy-start.3 = (bf16[2048,64]{0,1:T(8,128)(2,1)S(1)}, bf16[2048,64]{0,1:T(8,128)(2,1)}, u32[]{:S(2)}) copy-start(bf16[2048,64]{0,1:T(8,128)(2,1)} %param.16) | copy-start | bytes 786436
  7.2 23.0 %copy-start.4 = (bf16[2048,64]{0,1:T(8,128)(2,1)S(1)}, bf16[2048,64]{0,1:T(8,128)(2,1)}, u32[]{:S(2)}) copy-start(bf16[2048,64]{0,1:T(8,128)(2,1)} %param.17) | copy-start | bytes 786436
  7.2 29.0 %all-gather.2.cloned.1.call-start = ((), (), s32[]{:S(2)}) async-start(), calls=%async_computation.1 | async-start | bytes 1179648 | tf_op jit(solution)/shard_map/all_gather | solution.py:84
  8.0 115.7 %reduce-scatter.2.cloned.1.call-start = ((), (), s32[]{:S(2)}) async-start(), calls=%async_computation.2 | async-start | bytes 1179648 | tf_op jit(solution)/shard_map/reduce_scatter | solution.py:167
  28.6 7.6 %copy-start.7 = (f32[2048]{0:T(1024)S(1)}, f32[2048]{0:T(1024)}, u32[]{:S(2)}) copy-start(f32[2048]{0:T(1024)} %param.14) | copy-start | bytes 24580
  36.2 14.9 %copy-start.6 = (bf16[512,256]{1,0:T(8,128)(2,1)S(1)}, bf16[512,256]{1,0:T(8,128)(2,1)}, u32[]{:S(2)}) copy-start(bf16[512,256]{1,0:T(8,128)(2,1)} %param.19) | copy-start | bytes 786436
  36.2 14.9 %copy-start.8 = (f32[512]{0:T(512)S(1)}, f32[512]{0:T(512)}, u32[]{:S(2)}) copy-start(f32[512]{0:T(512)} %param.18) | copy-start | bytes 6148
  39.9 31.4 %collective-permute-start = (bf16[256,64]{0,1:T(8,128)(2,1)S(1)}, bf16[256,64]{0,1:T(8,128)(2,1)S(1)}, u32[]{:S(2)}, u32[]{:S(2)}) collective-permute-start(bf16[256,64]{0,1:T(8,128)(2,1)S(1)} %maximum_bitcast_fusion), channel_id=1, source_target_pairs={{0,8},{8,16},{16,24},{24,0},{1,9},{9,17},{17,25},{25,1},{2,10},{10... | collective-permute-start | bytes 98312 | tf_op jit(solution)/shard_map/ppermute | solution.py:128
  67.3 10.9 %collective-permute-start.3 = (bf16[1,128]{0,1:T(8,128)(2,1)S(1)}, bf16[1,128]{0,1:T(8,128)(2,1)S(1)}, u32[]{:S(2)}, u32[]{:S(2)}) collective-permute-start(bf16[1,128]{0,1:T(8,128)(2,1)S(1)} %get-tuple-element.26), channel_id=1, source_target_pairs={{0,8},{8,16},{16,24},{1,9},{9,17},{17,25},{2,10},{10,18},{18,26},{... | collective-permute-start | bytes 776 | tf_op jit(solution)/shard_map/ppermute | solution.py:23
  70.0 8.1 %collective-permute-start.4 = (bf16[1,128]{0,1:T(8,128)(2,1)S(1)}, bf16[1,128]{0,1:T(8,128)(2,1)S(1)}, u32[]{:S(2)}, u32[]{:S(2)}) collective-permute-start(bf16[1,128]{0,1:T(8,128)(2,1)S(1)} %get-tuple-element.36), channel_id=1, source_target_pairs={{8,0},{16,8},{24,16},{9,1},{17,9},{25,17},{10,2},{18,10},{26,18},{... | collective-permute-start | bytes 776 | tf_op jit(solution)/shard_map/ppermute | solution.py:24
  71.3 6.8 %collective-permute-start.1 = (bf16[256,64]{0,1:T(8,128)(2,1)S(1)}, bf16[256,64]{0,1:T(8,128)(2,1)S(1)}, u32[]{:S(2)}, u32[]{:S(2)}) collective-permute-start(bf16[256,64]{0,1:T(8,128)(2,1)S(1)} %collective-permute-done), channel_id=1, source_target_pairs={{0,8},{8,16},{16,24},{24,0},{1,9},{9,17},{17,25},{25,1},{2,10},{10... | collective-permute-start | bytes 98312 | tf_op jit(solution)/shard_map/ppermute | solution.py:128
  78.1 5.7 %collective-permute-start.2 = (bf16[256,64]{0,1:T(8,128)(2,1)S(1)}, bf16[256,64]{0,1:T(8,128)(2,1)S(1)}, u32[]{:S(2)}, u32[]{:S(2)}) collective-permute-start(bf16[256,64]{0,1:T(8,128)(2,1)S(1)} %collective-permute-done.1), channel_id=1, source_target_pairs={{0,8},{8,16},{16,24},{24,0},{1,9},{9,17},{17,25},{25,1},{2,10},{10... | collective-permute-start | bytes 98312 | tf_op jit(solution)/shard_map/ppermute | solution.py:128
  84.3 2.8 %copy-start.2 = (bf16[128,2048]{1,0:T(8,128)(2,1)S(1)}, bf16[128,2048]{1,0:T(8,128)(2,1)}, u32[]{:S(2)}) copy-start(bf16[128,2048]{1,0:T(8,128)(2,1)} %param.25) | copy-start | bytes 1572868
Sparse Core Ops, SparseCore 0:
  9.9 26.2 all-gather.1
  90.5 33.1 reduce-scatter.1
